TPU v7x, 32 devices: a whole 2x2x4 slice. The times are simulated.
32 devices in a mesh: sp: 8 (over z, x), tp: 4 (over y, core).
Axes of the slice: x: 2, y: 2, z: 4, core: 2. Of those that a mesh axis runs over, the one named last changes fastest.
Arguments:
- queries: bfloat16 [1024, 2048], P('sp', 'tp'), may hold values from -6 to 6
- keys: bfloat16 [1024, 512], P('sp', 'tp'), may hold values from -6 to 6
- values: bfloat16 [1024, 512], P('sp', 'tp'), may hold values from -6 to 6
- break_bias: float32 [16], P('tp'), as said below
- residual: bfloat16 [1024, 4096], P(('sp', 'tp')), may hold values from -6 to 6
- w_out: bfloat16 [2048, 4096], P('tp'), may hold values from -0.125 to 0.125
- ffn_gain: float32 [4096], replicated, may hold values from 0.1 to 1.9
- pick_ids: int32 [1024, 2], P('sp'), may hold values from 0 to 7, as said below
- pair_logit: float32 [1024], P('sp'), may hold values from -8 to 8
- w_gate: bfloat16 [8, 4096, 1024], P('sp', None, 'tp'), may hold values from -0.09375 to 0.09375
- w_up: bfloat16 [8, 4096, 1024], P('sp', None, 'tp'), may hold values from -0.09375 to 0.09375
- w_down: bfloat16 [8, 1024, 4096], P('sp', 'tp'), may hold values from -0.1875 to 0.1875
- out_gain: float32 [4096], replicated, may hold values from 0.1 to 1.9
Outputs:
- new_stream: bfloat16 [1024, 4096], P(('sp', 'tp'))
Inputs may be any that keep to these rules, and one draw needn't show every extreme that they name: `break_bias`: the logarithm of a break rate per position: between ln(0.02 / 1024) and ln(8 / 128). `pick_ids`: A row's 2 experts differ and lie in one group of 2 consecutive experts. In each aligned block of 32 rows no expert is named more than 12 times, and some expert exactly 12 times.
All inputs are finite; a program needn't handle non-finite values.
Results may differ from a plain program's by a relative error of at most 0.017.
Values may be sent and summed in bfloat16 or wider, within the bound.
A program may use at most 64 MiB of HBM per device.

v0:
```python
import jax
import jax.numpy as jnp
from jax import lax
from jax.sharding import PartitionSpec as P

HEAD = 128
TOP = 2
epsilon = 1e-06


def passed_along(block, axis, distance):
    devices = range(lax.axis_size(axis))
    route = [(i - distance, i) for i in devices if i - distance in devices]
    return lax.ppermute(block, axis, route)


def stick_block(carried, query_rows, key_block, value_block, head_bias, query_pos, key_pos, usable):
    output, used_up = carried
    scores = jnp.einsum("qcgd,scd->qcgs", query_rows, key_block, preferred_element_type=jnp.float32)
    scores = scores * query_rows.shape[-1] ** (-0.5) + head_bias[None, :, :, None]
    before = ((key_pos[None, :] < query_pos[:, None]) & usable)[:, None, None, :]
    breaks = jnp.where(before, jax.nn.softplus(scores), 0.0)
    behind = lax.cumsum(breaks, axis=3, reverse=True) - breaks
    weights = jnp.where(
        before, jnp.exp(jax.nn.log_sigmoid(scores) - behind - used_up[..., None]), 0.0
    )
    output = output + jnp.einsum(
        "qcgs,scd->qcgd",
        weights.astype(jnp.bfloat16),
        value_block,
        preferred_element_type=jnp.float32,
    )
    return (output, used_up + jnp.sum(breaks, axis=3))


def normed_heads(output):
    scaled = output * lax.rsqrt(jnp.mean(output * output, axis=-1, keepdims=True) + epsilon)
    return scaled.astype(jnp.bfloat16).reshape(output.shape[0], -1)


def on_device(
    queries,
    keys,
    values,
    break_bias,
    residual,
    w_out,
    ffn_gain,
    pick_ids,
    pair_logit,
    w_gate,
    w_up,
    w_down,
    out_gain,
):
    length = queries.shape[0]
    kv_local = keys.shape[1] // HEAD
    per_key = queries.shape[1] // keys.shape[1]
    query_rows = queries.reshape(length, kv_local, per_key, HEAD)
    head_bias = break_bias.reshape(kv_local, per_key)
    position = lax.axis_index("sp")
    offset = position * length
    query_pos = offset + jnp.arange(length, dtype=jnp.int32)
    initial = (
        jnp.zeros((length, kv_local, per_key, HEAD), jnp.float32),
        jnp.zeros((length, kv_local, per_key), jnp.float32),
    )
    stacked = jnp.stack([keys, values])
    carried = stick_block(
        initial,
        query_rows,
        keys.reshape(length, kv_local, HEAD),
        values.reshape(length, kv_local, HEAD),
        head_bias,
        query_pos,
        query_pos,
        True,
    )

    def visit(step_index, loop_state):
        arrived_pair, carried = loop_state
        arrived_pair = passed_along(arrived_pair, "sp", 1)
        source = position - step_index
        key_pos = source * length + jnp.arange(length, dtype=jnp.int32)
        carried = stick_block(
            carried,
            query_rows,
            arrived_pair[0].reshape(length, kv_local, HEAD),
            arrived_pair[1].reshape(length, kv_local, HEAD),
            head_bias,
            query_pos,
            key_pos,
            source >= 0,
        )
        return (arrived_pair, carried)

    head_out = normed_heads(lax.fori_loop(1, lax.axis_size("sp"), visit, (stacked, carried))[1][0])
    quarters = lax.axis_size("tp")
    quarter = lax.axis_index("tp")
    slice_rows = length // quarters
    width = w_out.shape[1]
    experts = lax.axis_size("sp")
    capacity = max(2, (3 * slice_rows + experts - 1) // experts)
    mixed = lax.psum_scatter(
        jnp.dot(head_out, w_out, preferred_element_type=jnp.float32).astype(jnp.bfloat16),
        "tp",
        scatter_dimension=0,
        tiled=True,
    ).astype(jnp.float32)
    stream = (residual.astype(jnp.float32) + mixed).astype(jnp.bfloat16)
    routed = lax.dynamic_slice_in_dim(pick_ids, quarter * slice_rows, slice_rows, 0)[None]
    stream_float = stream.astype(jnp.float32)
    ffn_in = (
        stream_float
        * lax.rsqrt(jnp.mean(stream_float * stream_float, axis=-1, keepdims=True) + epsilon)
        * ffn_gain
    ).astype(jnp.bfloat16)
    blocks = routed.shape[0]
    entries = ffn_in.reshape(blocks, slice_rows, width)
    flat_ids = routed.reshape(blocks, slice_rows * TOP)
    places = jnp.arange(slice_rows * TOP, dtype=jnp.int32)
    earlier = places[None, :] < places[:, None]
    matches = (flat_ids[:, :, None] == flat_ids[:, None, :]) & earlier[None]
    ranks = jnp.sum(matches.astype(jnp.int32), axis=2)
    targets = (flat_ids * capacity + ranks).reshape(blocks, slice_rows, TOP)
    block_ids = jnp.arange(blocks, dtype=jnp.int32)[:, None]
    outgoing = jnp.zeros((blocks, experts * capacity, width), jnp.bfloat16)
    for pick_index in range(TOP):
        outgoing = outgoing.at[block_ids, targets[:, :, pick_index]].set(entries)
    arrived = lax.all_to_all(outgoing, "sp", split_axis=1, concat_axis=1, tiled=True).reshape(
        -1, width
    )
    piece = lax.all_gather(arrived, "tp", axis=0, tiled=True)
    gated = jax.nn.silu(jnp.dot(piece, w_gate[0], preferred_element_type=jnp.float32))
    hidden = (gated * jnp.dot(piece, w_up[0], preferred_element_type=jnp.float32)).astype(
        jnp.bfloat16
    )
    results = lax.psum_scatter(
        jnp.dot(hidden, w_down[0], preferred_element_type=jnp.float32).astype(jnp.bfloat16),
        "tp",
        scatter_dimension=0,
        tiled=True,
    )
    returned = lax.all_to_all(results, "sp", split_axis=0, concat_axis=0, tiled=True)
    own_targets = targets[0]
    logits = lax.dynamic_slice_in_dim(pair_logit, quarter * slice_rows, slice_rows, 0)
    leading = returned[own_targets[:, 0]].astype(jnp.float32)
    trailing = returned[own_targets[:, 1]].astype(jnp.float32)
    blended = (
        jax.nn.sigmoid(logits)[:, None] * leading + jax.nn.sigmoid(-logits)[:, None] * trailing
    )
    blend_scale = lax.rsqrt(jnp.mean(blended * blended, axis=-1, keepdims=True) + epsilon)
    return (stream_float + blended * blend_scale * out_gain).astype(jnp.bfloat16)


def solution(mesh):
    placed = (
        P("sp", "tp"),
        P("sp", "tp"),
        P("sp", "tp"),
        P("tp"),
        P(("sp", "tp"), None),
        P("tp", None),
        P(),
        P("sp", None),
        P("sp"),
        P("sp", None, "tp"),
        P("sp", None, "tp"),
        P("sp", "tp", None),
        P(),
    )
    return jax.shard_map(
        on_device, mesh=mesh, in_specs=placed, out_specs=P(("sp", "tp"), None), check_vma=False
    )
```

profile of v0, /device:TPU:0, one launch (start us, length us, event | category | flops | bytes accessed | tf_op | source)
XLA Modules:
  0.0 276.8 jit_solution(1136986469250857039)
XLA Ops:
  11.0 62.2 %while.18 = (s32[]{:T(128)}, bf16[2,128,128]{2,1,0:T(8,128)(2,1)S(1)}, f32[128,1,4,128]{3,0,2,1:T(8,128)S(1)}, f32[128,1,4]{0,2,1:T(4,128)S(1)}, s32[]{:T(128)},...) while((s32[]{:T(128)}, ...), condition=%wide.region_5.6_spmd.clone, body=%wide.region_2.5_spmd.clone.sunk | while | flops 43942148 | bytes 2749119 | solution.py:97
  11.0 4.9 %collective-permute-start = (bf16[2,128,128]{2,1,0:T(8,128)(2,1)S(1)}, bf16[2,128,128]{2,1,0:T(8,128)(2,1)S(1)}, u32[]{:S(2)}, u32[]{:S(2)}) collective-permute-start(bf16[2,128,128]{2,1,0:T(8,128)(2,1)S(1)} %get-tuple-element.307), channel_id=1, source_target_pairs={{0,4},{4,8},{8,12},{12,16},{16,20},{20,24},{24,28},{1,5},{5,9},{9,... | collective-permute-start | bytes 196616 | tf_op jit(solution)/shard_map/while/body/eval_jaxpr/ppermute | solution.py:14
  19.9 4.3 %collective-permute-start = (bf16[2,128,128]{2,1,0:T(8,128)(2,1)S(1)}, bf16[2,128,128]{2,1,0:T(8,128)(2,1)S(1)}, u32[]{:S(2)}, u32[]{:S(2)}) collective-permute-start(bf16[2,128,128]{2,1,0:T(8,128)(2,1)S(1)} %get-tuple-element.307), channel_id=1, source_target_pairs={{0,4},{4,8},{8,12},{12,16},{16,20},{20,24},{24,28},{1,5},{5,9},{9,... | collective-permute-start | bytes 196616 | tf_op jit(solution)/shard_map/while/body/eval_jaxpr/ppermute | solution.py:14
  28.2 4.4 %collective-permute-start = (bf16[2,128,128]{2,1,0:T(8,128)(2,1)S(1)}, bf16[2,128,128]{2,1,0:T(8,128)(2,1)S(1)}, u32[]{:S(2)}, u32[]{:S(2)}) collective-permute-start(bf16[2,128,128]{2,1,0:T(8,128)(2,1)S(1)} %get-tuple-element.307), channel_id=1, source_target_pairs={{0,4},{4,8},{8,12},{12,16},{16,20},{20,24},{24,28},{1,5},{5,9},{9,... | collective-permute-start | bytes 196616 | tf_op jit(solution)/shard_map/while/body/eval_jaxpr/ppermute | solution.py:14
  32.6 1.8 collective-permute-done
  36.5 5.2 %collective-permute-start = (bf16[2,128,128]{2,1,0:T(8,128)(2,1)S(1)}, bf16[2,128,128]{2,1,0:T(8,128)(2,1)S(1)}, u32[]{:S(2)}, u32[]{:S(2)}) collective-permute-start(bf16[2,128,128]{2,1,0:T(8,128)(2,1)S(1)} %get-tuple-element.307), channel_id=1, source_target_pairs={{0,4},{4,8},{8,12},{12,16},{16,20},{20,24},{24,28},{1,5},{5,9},{9,... | collective-permute-start | bytes 196616 | tf_op jit(solution)/shard_map/while/body/eval_jaxpr/ppermute | solution.py:14
  45.7 5.2 %collective-permute-start = (bf16[2,128,128]{2,1,0:T(8,128)(2,1)S(1)}, bf16[2,128,128]{2,1,0:T(8,128)(2,1)S(1)}, u32[]{:S(2)}, u32[]{:S(2)}) collective-permute-start(bf16[2,128,128]{2,1,0:T(8,128)(2,1)S(1)} %get-tuple-element.307), channel_id=1, source_target_pairs={{0,4},{4,8},{8,12},{12,16},{16,20},{20,24},{24,28},{1,5},{5,9},{9,... | collective-permute-start | bytes 196616 | tf_op jit(solution)/shard_map/while/body/eval_jaxpr/ppermute | solution.py:14
  54.9 5.2 %collective-permute-start = (bf16[2,128,128]{2,1,0:T(8,128)(2,1)S(1)}, bf16[2,128,128]{2,1,0:T(8,128)(2,1)S(1)}, u32[]{:S(2)}, u32[]{:S(2)}) collective-permute-start(bf16[2,128,128]{2,1,0:T(8,128)(2,1)S(1)} %get-tuple-element.307), channel_id=1, source_target_pairs={{0,4},{4,8},{8,12},{12,16},{16,20},{20,24},{24,28},{1,5},{5,9},{9,... | collective-permute-start | bytes 196616 | tf_op jit(solution)/shard_map/while/body/eval_jaxpr/ppermute | solution.py:14
  64.1 5.2 %collective-permute-start = (bf16[2,128,128]{2,1,0:T(8,128)(2,1)S(1)}, bf16[2,128,128]{2,1,0:T(8,128)(2,1)S(1)}, u32[]{:S(2)}, u32[]{:S(2)}) collective-permute-start(bf16[2,128,128]{2,1,0:T(8,128)(2,1)S(1)} %get-tuple-element.307), channel_id=1, source_target_pairs={{0,4},{4,8},{8,12},{12,16},{16,20},{20,24},{24,28},{1,5},{5,9},{9,... | collective-permute-start | bytes 196616 | tf_op jit(solution)/shard_map/while/body/eval_jaxpr/ppermute | solution.py:14
  73.6 4.0 %convolution_convert_fusion.1 = bf16[128,4096]{1,0:T(8,128)(2,1)} fusion(bf16[128,512]{0,1:T(8,128)(2,1)S(1)} %bitcast.134, bf16[512,4096]{1,0:T(8,128)(2,1)} %param.20), kind=kOutput, calls=%fused_computation.36 | convolution fusion | flops 537395200 | bytes 5373952 | tf_op jit(solution)/shard_map/dot_general | solution.py:105
  78.9 27.4 %reduce-scatter.3.cloned.1.call-done = bf16[32,4096]{1,0:T(8,128)(2,1)} async-done(((bf16[128,4096]{1,0:T(8,128)(2,1)}), bf16[32,4096]{1,0:T(8,128)(2,1)}) %reduce-scatter.3.cloned.1.call-update) | async-done | bytes 262160 | tf_op jit(solution)/shard_map/reduce_scatter | solution.py:104
  110.6 2.9 %copy.126 = bf16[1,96,4096]{2,0,1:T(2,128)(2,1)} copy(bf16[1,96,4096]{2,1,0:T(8,128)(2,1)S(1)} %bitcast.132) | data formatting | bytes 1572864 | tf_op jit(solution)/shard_map/scatter | solution.py:129
  114.0 6.7 %reduce.14 = bf16[96,4096]{1,0:T(8,128)(2,1)S(1)} reduce(bf16[96,1,4096]{2,1,0:T(2,128)(2,1)} %bitcast.130, bf16[]{:T(256)} %broadcast.261), dimensions={1}, to_apply=%bitcast.113.reduce_sub_computation | reduce | bytes 1572866
  122.3 25.5 %all_to_all.17 = bf16[8,2,24576]{2,1,0:T(2,128)(2,1)S(1)} all-to-all(bf16[8,2,24576]{2,1,0:T(2,128)(2,1)} %reshape.361), channel_id=1, replica_groups=mesh['sp'=8,'tp'=4] {'sp'}, dimensions={0} | all-to-all | bytes 1572864 | tf_op jit(solution)/shard_map/all_to_all | solution.py:130
  147.8 3.2 %reshape.362 = bf16[96,1,4096]{2,1,0:T(2,128)(2,1)} reshape(bf16[8,2,24576]{2,1,0:T(2,128)(2,1)S(1)} %all_to_all.17) | data formatting | bytes 1572864
  150.9 3.1 %copy.94 = bf16[1,96,4096]{2,1,0:T(8,128)(2,1)} copy(bf16[1,96,4096]{2,0,1:T(2,128)(2,1)} %bitcast.131) | data formatting | bytes 1572864 | tf_op jit(solution)/shard_map/all_to_all | solution.py:130
  154.2 26.7 %all-gather.3.cloned.1.call-done = bf16[1,384,4096]{2,1,0:T(8,128)(2,1)} async-done(((bf16[1,96,4096]{2,1,0:T(8,128)(2,1)}), bf16[1,384,4096]{2,1,0:T(8,128)(2,1)}) %all-gather.3.cloned.1.call-update) | async-done | bytes 3145744 | tf_op jit(solution)/shard_map/all_gather | solution.py:133
  180.9 3.5 %fusion.25 = f32[384,256]{1,0:T(8,128)S(1)} fusion(bf16[1,384,4096]{2,1,0:T(8,128)(2,1)} %all-gather.3.cloned.1.call-done, bf16[1,4096,256]{2,1,0:T(8,128)(2,1)} %param.24), kind=kOutput, calls=%fused_computation.39 | convolution fusion | flops 805306368 | bytes 5636096 | tf_op jit(solution)/shard_map/dot_general | solution.py:134
  184.4 7.7 %convolution_convert_fusion = bf16[384,4096]{1,0:T(8,128)(2,1)} fusion(bf16[1,256,4096]{2,1,0:T(8,128)(2,1)S(1)} %copy-done, bf16[1,4096,256]{2,1,0:T(8,128)(2,1)} %param.25, bf16[1,384,4096]{2,1,0:T(8,128)(2,1)} %all-gather.3.cloned.1.call-done, f32[384,256]{1,0:T(8,128)S(1)} %fusion.25), kind=kOutput, calls=%fused_computation.35 | convolution fusion | flops 1612775424 | bytes 10878976 | tf_op jit(solution)/shard_map/dot_general | solution.py:139
  192.1 38.0 %reduce-scatter.5.cloned.1.call-done = bf16[96,4096]{1,0:T(8,128)(2,1)} async-done(((bf16[384,4096]{1,0:T(8,128)(2,1)}), bf16[96,4096]{1,0:T(8,128)(2,1)}) %reduce-scatter.5.cloned.1.call-update) | async-done | bytes 786448 | tf_op jit(solution)/shard_map/reduce_scatter | solution.py:138
  230.2 2.2 all_to_all.12
  232.3 5.5 %all-to-all-start.1 = ((bf16[8,12,4096]{2,1,0:T(8,128)(2,1)}), bf16[8,12,4096]{2,1,0:T(8,128)(2,1)}, u32[]{:S(2)}, u32[]{:S(2)}) async-start(bf16[8,12,4096]{2,1,0:T(8,128)(2,1)} %all_to_all.12), calls=%async_computation.3 | async-start | bytes 2097152 | tf_op jit(solution)/shard_map/all_to_all | solution.py:144
  238.1 25.5 %all-to-all-done.1 = bf16[8,12,4096]{2,1,0:T(8,128)(2,1)} async-done(((bf16[8,12,4096]{2,1,0:T(8,128)(2,1)}), bf16[8,12,4096]{2,1,0:T(8,128)(2,1)}, u32[]{:S(2)}, u32[]{:S(2)}) %all-to-all-start.1) | async-done | bytes 786464 | tf_op jit(solution)/shard_map/all_to_all | solution.py:144
  268.4 1.9 fusion.50
  (122 shorter events, 43.2 us)
Async XLA Ops:
  6.5 177.9 %copy-start = (bf16[1,256,4096]{2,1,0:T(8,128)(2,1)S(1)}, bf16[1,256,4096]{2,1,0:T(8,128)(2,1)}, u32[]{:S(2)}) copy-start(bf16[1,256,4096]{2,1,0:T(8,128)(2,1)} %param.26) | copy-start | bytes 6291460
  6.5 4.5 %copy-start.8 = (f32[4]{0:T(128)S(1)}, f32[4]{0:T(128)}, u32[]{:S(2)}) copy-start(f32[4]{0:T(128)} %param.18) | copy-start | bytes 52
  6.5 3.9 %copy-start.3 = (bf16[128,128]{1,0:T(8,128)(2,1)S(1)}, bf16[128,128]{1,0:T(8,128)(2,1)}, u32[]{:S(2)}) copy-start(bf16[128,128]{1,0:T(8,128)(2,1)} %param.16) | copy-start | bytes 98308
  6.5 3.9 %copy-start.4 = (bf16[128,128]{1,0:T(8,128)(2,1)S(1)}, bf16[128,128]{1,0:T(8,128)(2,1)}, u32[]{:S(2)}) copy-start(bf16[128,128]{1,0:T(8,128)(2,1)} %param.17) | copy-start | bytes 98308
  6.5 99.8 %reduce-scatter.3.cloned.1.call-start = ((), (), s32[]{:S(2)}) async-start(), calls=%async_computation.4 | async-start | bytes 1310720 | tf_op jit(solution)/shard_map/reduce_scatter | solution.py:104
  11.0 6.8 %collective-permute-start = (bf16[2,128,128]{2,1,0:T(8,128)(2,1)S(1)}, bf16[2,128,128]{2,1,0:T(8,128)(2,1)S(1)}, u32[]{:S(2)}, u32[]{:S(2)}) collective-permute-start(bf16[2,128,128]{2,1,0:T(8,128)(2,1)S(1)} %get-tuple-element.307), channel_id=1, source_target_pairs={{0,4},{4,8},{8,12},{12,16},{16,20},{20,24},{24,28},{1,5},{5,9},{9,... | collective-permute-start | bytes 196616 | tf_op jit(solution)/shard_map/while/body/eval_jaxpr/ppermute | solution.py:14
  19.9 6.2 %collective-permute-start = (bf16[2,128,128]{2,1,0:T(8,128)(2,1)S(1)}, bf16[2,128,128]{2,1,0:T(8,128)(2,1)S(1)}, u32[]{:S(2)}, u32[]{:S(2)}) collective-permute-start(bf16[2,128,128]{2,1,0:T(8,128)(2,1)S(1)} %get-tuple-element.307), channel_id=1, source_target_pairs={{0,4},{4,8},{8,12},{12,16},{16,20},{20,24},{24,28},{1,5},{5,9},{9,... | collective-permute-start | bytes 196616 | tf_op jit(solution)/shard_map/while/body/eval_jaxpr/ppermute | solution.py:14
  28.2 6.2 %collective-permute-start = (bf16[2,128,128]{2,1,0:T(8,128)(2,1)S(1)}, bf16[2,128,128]{2,1,0:T(8,128)(2,1)S(1)}, u32[]{:S(2)}, u32[]{:S(2)}) collective-permute-start(bf16[2,128,128]{2,1,0:T(8,128)(2,1)S(1)} %get-tuple-element.307), channel_id=1, source_target_pairs={{0,4},{4,8},{8,12},{12,16},{16,20},{20,24},{24,28},{1,5},{5,9},{9,... | collective-permute-start | bytes 196616 | tf_op jit(solution)/shard_map/while/body/eval_jaxpr/ppermute | solution.py:14
  36.5 7.1 %collective-permute-start = (bf16[2,128,128]{2,1,0:T(8,128)(2,1)S(1)}, bf16[2,128,128]{2,1,0:T(8,128)(2,1)S(1)}, u32[]{:S(2)}, u32[]{:S(2)}) collective-permute-start(bf16[2,128,128]{2,1,0:T(8,128)(2,1)S(1)} %get-tuple-element.307), channel_id=1, source_target_pairs={{0,4},{4,8},{8,12},{12,16},{16,20},{20,24},{24,28},{1,5},{5,9},{9,... | collective-permute-start | bytes 196616 | tf_op jit(solution)/shard_map/while/body/eval_jaxpr/ppermute | solution.py:14
  45.7 7.1 %collective-permute-start = (bf16[2,128,128]{2,1,0:T(8,128)(2,1)S(1)}, bf16[2,128,128]{2,1,0:T(8,128)(2,1)S(1)}, u32[]{:S(2)}, u32[]{:S(2)}) collective-permute-start(bf16[2,128,128]{2,1,0:T(8,128)(2,1)S(1)} %get-tuple-element.307), channel_id=1, source_target_pairs={{0,4},{4,8},{8,12},{12,16},{16,20},{20,24},{24,28},{1,5},{5,9},{9,... | collective-permute-start | bytes 196616 | tf_op jit(solution)/shard_map/while/body/eval_jaxpr/ppermute | solution.py:14
  54.9 7.1 %collective-permute-start = (bf16[2,128,128]{2,1,0:T(8,128)(2,1)S(1)}, bf16[2,128,128]{2,1,0:T(8,128)(2,1)S(1)}, u32[]{:S(2)}, u32[]{:S(2)}) collective-permute-start(bf16[2,128,128]{2,1,0:T(8,128)(2,1)S(1)} %get-tuple-element.307), channel_id=1, source_target_pairs={{0,4},{4,8},{8,12},{12,16},{16,20},{20,24},{24,28},{1,5},{5,9},{9,... | collective-permute-start | bytes 196616 | tf_op jit(solution)/shard_map/while/body/eval_jaxpr/ppermute | solution.py:14
  64.1 7.1 %collective-permute-start = (bf16[2,128,128]{2,1,0:T(8,128)(2,1)S(1)}, bf16[2,128,128]{2,1,0:T(8,128)(2,1)S(1)}, u32[]{:S(2)}, u32[]{:S(2)}) collective-permute-start(bf16[2,128,128]{2,1,0:T(8,128)(2,1)S(1)} %get-tuple-element.307), channel_id=1, source_target_pairs={{0,4},{4,8},{8,12},{12,16},{16,20},{20,24},{24,28},{1,5},{5,9},{9,... | collective-permute-start | bytes 196616 | tf_op jit(solution)/shard_map/while/body/eval_jaxpr/ppermute | solution.py:14
  73.6 4.1 %copy-start.6 = (s32[128,2]{0,1:T(2,128)S(1)}, s32[128,2]{0,1:T(2,128)}, u32[]{:S(2)}) copy-start(s32[128,2]{0,1:T(2,128)} %param.22) | copy-start | bytes 3076
  73.6 32.8 %copy-start.1 = (bf16[32,4096]{1,0:T(8,128)(2,1)S(1)}, bf16[32,4096]{1,0:T(8,128)(2,1)}, u32[]{:S(2)}) copy-start(bf16[32,4096]{1,0:T(8,128)(2,1)} %param.19) | copy-start | bytes 786436
  77.6 30.0 %copy-start.2 = (f32[4096]{0:T(1024)S(1)}, f32[4096]{0:T(1024)}, u32[]{:S(2)}) copy-start(f32[4096]{0:T(1024)} %param.21) | copy-start | bytes 49156
  77.6 103.3 %all-gather.3.cloned.1.call-start = ((), (), s32[]{:S(2)}) async-start(), calls=%async_computation.6 | async-start | bytes 3932160 | tf_op jit(solution)/shard_map/all_gather | solution.py:133
  154.1 76.0 %reduce-scatter.5.cloned.1.call-start = ((), (), s32[]{:S(2)}) async-start(), calls=%async_computation.5 | async-start | bytes 3932160 | tf_op jit(solution)/shard_map/reduce_scatter | solution.py:138
  192.1 45.8 %copy-start.7 = (f32[128]{0:T(128)S(1)}, f32[128]{0:T(128)}, u32[]{:S(2)}) copy-start(f32[128]{0:T(128)} %param.23) | copy-start | bytes 1540
  232.3 31.3 %all-to-all-start.1 = ((bf16[8,12,4096]{2,1,0:T(8,128)(2,1)}), bf16[8,12,4096]{2,1,0:T(8,128)(2,1)}, u32[]{:S(2)}, u32[]{:S(2)}) async-start(bf16[8,12,4096]{2,1,0:T(8,128)(2,1)} %all_to_all.12), calls=%async_computation.3 | async-start | bytes 2097152 | tf_op jit(solution)/shard_map/all_to_all | solution.py:144
  265.0 3.4 %copy-start.5 = (f32[4096]{0:T(1024)S(1)}, f32[4096]{0:T(1024)}, u32[]{:S(2)}) copy-start(f32[4096]{0:T(1024)} %param.27) | copy-start | bytes 49156
Sparse Core Ops, SparseCore 0:
  77.7 28.6 reduce-scatter.2
  154.2 26.5 all-gather.2
  192.2 37.8 reduce-scatter.4
where the time goes:
time: 277 us
  waiting for transfers between devices  130 us (47%)
  starting transfers between devices  39.8 us (14%)
  blocking collectives  25.5 us (9%)
  other arithmetic  24.8 us (9%)
  matrix products  23.4 us (8%)
  local copies, waits for them, and re-layouts  19.4 us (7%)
  between operations  13.4 us (5%)
    reduce_scatter x1, waiting for transfers between devices, on_device(): lax.psum_scatter(jnp.dot(hidden, w_down[0], preferred_element_type=jnp.fl...  38 us
    ppermute x7, starting transfers between devices, passed_along(): return lax.ppermute(block, axis, route)  34.2 us
    reduce_scatter x1, waiting for transfers between devices, on_device(): lax.psum_scatter(jnp.dot(head_out, w_out, preferred_element_type=jnp.floa...  27.4 us
    all_gather x1, waiting for transfers between devices, on_device(): piece = lax.all_gather(arrived, 'tp', axis=0, tiled=True)  26.7 us
    all_to_all x1, waiting for transfers between devices, on_device(): lax.all_to_all(results, 'sp', split_axis=0, concat_axis=0, tiled=True)  25.5 us
    all_to_all x1, blocking collectives, on_device(): lax.all_to_all(outgoing, 'sp', split_axis=1, concat_axis=1, tiled=True)  25.5 us
    ppermute x7, waiting for transfers between devices, passed_along(): return lax.ppermute(block, axis, route)  12.4 us
    another operation x8, other arithmetic, stick_block(): behind = lax.cumsum(breaks, axis=3, reverse=True) - breaks  9.21 us
  transfers between devices with their start and end apart: 11, of which 11 were waited for; matrix products, arithmetic and copies ran while one was open for 1% of the time, Pallas kernels for 0%

commit v1 on v0

--- a/solution.py
+++ b/solution.py
@@ -6,6 +6,12 @@
 HEAD = 128
 TOP = 2
 epsilon = 1e-06
+
+
+def swap_blocks(array, axis, split, join):
+    pieces = jnp.split(array, lax.axis_size(axis), axis=split)
+    got = lax.all_to_all(jnp.stack(pieces), axis, 0, 0)
+    return jnp.concatenate(got, axis=join)
 
 
 def passed_along(block, axis, distance):
@@ -127,9 +133,7 @@
     outgoing = jnp.zeros((blocks, experts * capacity, width), jnp.bfloat16)
     for pick_index in range(TOP):
         outgoing = outgoing.at[block_ids, targets[:, :, pick_index]].set(entries)
-    arrived = lax.all_to_all(outgoing, "sp", split_axis=1, concat_axis=1, tiled=True).reshape(
-        -1, width
-    )
+    arrived = swap_blocks(outgoing, "sp", 1, 1).reshape(-1, width)
     piece = lax.all_gather(arrived, "tp", axis=0, tiled=True)
     gated = jax.nn.silu(jnp.dot(piece, w_gate[0], preferred_element_type=jnp.float32))
     hidden = (gated * jnp.dot(piece, w_up[0], preferred_element_type=jnp.float32)).astype(

time: 277 us -> 267 us (0.964)
  local copies, waits for them, and re-layouts: 19.4 us -> 9.24 us
  other arithmetic: 24.8 us -> 18.7 us
  blocking collectives: 25.5 us -> 30.9 us
    unnamed x1 -> x0, other arithmetic: 6.65 us -> none
    all_to_all x1, blocking collectives: 25.5 us -> 30.9 us  [swap_blocks(): got = lax.all_to_all(jnp.stack(pieces), axis, 0, 0)]
    unnamed x28, local copies, waits for them, and re-layouts: 7.1 us -> 1.93 us
    all_to_all x1 -> x0, local copies, waits for them, and re-layouts: 3.15 us -> none  [on_device(): lax.all_to_all(outgoing, 'sp', split_axis=1, concat_axis=1, tiled=True)]
    scatter x1 -> x0, local copies, waits for them, and re-layouts: 2.91 us -> none  [on_device(): outgoing = outgoing.at[block_ids, targets[:, :, pick_index]].set(entries)]
where the time goes in v1:
time: 267 us
  waiting for transfers between devices  130 us (49%)
  starting transfers between devices  39.9 us (15%)
  blocking collectives  30.9 us (12%)
  matrix products  24.1 us (9%)
  other arithmetic  18.7 us (7%)
  between operations  13.4 us (5%)
  local copies, waits for them, and re-layouts  9.24 us (3%)
    reduce_scatter x1, waiting for transfers between devices, on_device(): lax.psum_scatter(jnp.dot(hidden, w_down[0], preferred_element_type=jnp.fl...  38 us
    ppermute x7, starting transfers between devices, passed_along(): return lax.ppermute(block, axis, route)  34.2 us
    all_to_all x1, blocking collectives, swap_blocks(): got = lax.all_to_all(jnp.stack(pieces), axis, 0, 0)  30.9 us
    reduce_scatter x1, waiting for transfers between devices, on_device(): lax.psum_scatter(jnp.dot(head_out, w_out, preferred_element_type=jnp.floa...  27.4 us
    all_gather x1, waiting for transfers between devices, on_device(): piece = lax.all_gather(arrived, 'tp', axis=0, tiled=True)  26.5 us
    all_to_all x1, waiting for transfers between devices, on_device(): lax.all_to_all(results, 'sp', split_axis=0, concat_axis=0, tiled=True)  25.5 us
    ppermute x7, waiting for transfers between devices, passed_along(): return lax.ppermute(block, axis, route)  12.4 us
    another operation x8, other arithmetic, stick_block(): behind = lax.cumsum(breaks, axis=3, reverse=True) - breaks  9.21 us
  transfers between devices with their start and end apart: 11, of which 11 were waited for; matrix products, arithmetic and copies ran while one was open for 1% of the time, Pallas kernels for 0%

profile of v1, /device:TPU:0, one launch (start us, length us, event | category | flops | bytes accessed | tf_op | source)
XLA Modules:
  0.0 266.7 jit_solution(14858983805950094947)
XLA Ops:
  12.5 62.2 %while.18 = (s32[]{:T(128)}, bf16[2,128,128]{2,1,0:T(8,128)(2,1)S(1)}, f32[128,1,4,128]{3,0,2,1:T(8,128)S(1)}, f32[128,1,4]{0,2,1:T(4,128)S(1)}, s32[]{:T(128)},...) while((s32[]{:T(128)}, ...), condition=%wide.region_5.6_spmd.clone, body=%wide.region_2.5_spmd.clone.sunk | while | flops 43942148 | bytes 2749119 | solution.py:103
  12.5 4.9 %collective-permute-start = (bf16[2,128,128]{2,1,0:T(8,128)(2,1)S(1)}, bf16[2,128,128]{2,1,0:T(8,128)(2,1)S(1)}, u32[]{:S(2)}, u32[]{:S(2)}) collective-permute-start(bf16[2,128,128]{2,1,0:T(8,128)(2,1)S(1)} %get-tuple-element.299), channel_id=1, source_target_pairs={{0,4},{4,8},{8,12},{12,16},{16,20},{20,24},{24,28},{1,5},{5,9},{9,... | collective-permute-start | bytes 196616 | tf_op jit(solution)/shard_map/while/body/eval_jaxpr/ppermute | solution.py:20
  17.5 1.8 collective-permute-done
  21.3 4.3 %collective-permute-start = (bf16[2,128,128]{2,1,0:T(8,128)(2,1)S(1)}, bf16[2,128,128]{2,1,0:T(8,128)(2,1)S(1)}, u32[]{:S(2)}, u32[]{:S(2)}) collective-permute-start(bf16[2,128,128]{2,1,0:T(8,128)(2,1)S(1)} %get-tuple-element.299), channel_id=1, source_target_pairs={{0,4},{4,8},{8,12},{12,16},{16,20},{20,24},{24,28},{1,5},{5,9},{9,... | collective-permute-start | bytes 196616 | tf_op jit(solution)/shard_map/while/body/eval_jaxpr/ppermute | solution.py:20
  25.7 1.8 collective-permute-done
  29.6 4.4 %collective-permute-start = (bf16[2,128,128]{2,1,0:T(8,128)(2,1)S(1)}, bf16[2,128,128]{2,1,0:T(8,128)(2,1)S(1)}, u32[]{:S(2)}, u32[]{:S(2)}) collective-permute-start(bf16[2,128,128]{2,1,0:T(8,128)(2,1)S(1)} %get-tuple-element.299), channel_id=1, source_target_pairs={{0,4},{4,8},{8,12},{12,16},{16,20},{20,24},{24,28},{1,5},{5,9},{9,... | collective-permute-start | bytes 196616 | tf_op jit(solution)/shard_map/while/body/eval_jaxpr/ppermute | solution.py:20
  34.1 1.8 collective-permute-done
  38.0 5.2 %collective-permute-start = (bf16[2,128,128]{2,1,0:T(8,128)(2,1)S(1)}, bf16[2,128,128]{2,1,0:T(8,128)(2,1)S(1)}, u32[]{:S(2)}, u32[]{:S(2)}) collective-permute-start(bf16[2,128,128]{2,1,0:T(8,128)(2,1)S(1)} %get-tuple-element.299), channel_id=1, source_target_pairs={{0,4},{4,8},{8,12},{12,16},{16,20},{20,24},{24,28},{1,5},{5,9},{9,... | collective-permute-start | bytes 196616 | tf_op jit(solution)/shard_map/while/body/eval_jaxpr/ppermute | solution.py:20
  47.2 5.2 %collective-permute-start = (bf16[2,128,128]{2,1,0:T(8,128)(2,1)S(1)}, bf16[2,128,128]{2,1,0:T(8,128)(2,1)S(1)}, u32[]{:S(2)}, u32[]{:S(2)}) collective-permute-start(bf16[2,128,128]{2,1,0:T(8,128)(2,1)S(1)} %get-tuple-element.299), channel_id=1, source_target_pairs={{0,4},{4,8},{8,12},{12,16},{16,20},{20,24},{24,28},{1,5},{5,9},{9,... | collective-permute-start | bytes 196616 | tf_op jit(solution)/shard_map/while/body/eval_jaxpr/ppermute | solution.py:20
  52.5 1.8 collective-permute-done
  56.4 5.2 %collective-permute-start = (bf16[2,128,128]{2,1,0:T(8,128)(2,1)S(1)}, bf16[2,128,128]{2,1,0:T(8,128)(2,1)S(1)}, u32[]{:S(2)}, u32[]{:S(2)}) collective-permute-start(bf16[2,128,128]{2,1,0:T(8,128)(2,1)S(1)} %get-tuple-element.299), channel_id=1, source_target_pairs={{0,4},{4,8},{8,12},{12,16},{16,20},{20,24},{24,28},{1,5},{5,9},{9,... | collective-permute-start | bytes 196616 | tf_op jit(solution)/shard_map/while/body/eval_jaxpr/ppermute | solution.py:20
  61.6 1.8 collective-permute-done
  65.5 5.2 %collective-permute-start = (bf16[2,128,128]{2,1,0:T(8,128)(2,1)S(1)}, bf16[2,128,128]{2,1,0:T(8,128)(2,1)S(1)}, u32[]{:S(2)}, u32[]{:S(2)}) collective-permute-start(bf16[2,128,128]{2,1,0:T(8,128)(2,1)S(1)} %get-tuple-element.299), channel_id=1, source_target_pairs={{0,4},{4,8},{8,12},{12,16},{16,20},{20,24},{24,28},{1,5},{5,9},{9,... | collective-permute-start | bytes 196616 | tf_op jit(solution)/shard_map/while/body/eval_jaxpr/ppermute | solution.py:20
  75.1 4.0 %convolution_convert_fusion.1 = bf16[128,4096]{1,0:T(8,128)(2,1)} fusion(bf16[128,512]{0,1:T(8,128)(2,1)S(1)} %bitcast.158, bf16[512,4096]{1,0:T(8,128)(2,1)} %param.20), kind=kOutput, calls=%fused_computation.36 | convolution fusion | flops 537395200 | bytes 5373952 | tf_op jit(solution)/shard_map/dot_general | solution.py:111
  80.4 27.4 %reduce-scatter.3.cloned.1.call-done = bf16[32,4096]{1,0:T(8,128)(2,1)} async-done(((bf16[128,4096]{1,0:T(8,128)(2,1)}), bf16[32,4096]{1,0:T(8,128)(2,1)}) %reduce-scatter.3.cloned.1.call-update) | async-done | bytes 262160 | tf_op jit(solution)/shard_map/reduce_scatter | solution.py:110
  112.1 30.9 %all_to_all.17 = bf16[8,1,12,4096]{3,2,1,0:T(8,128)(2,1)S(1)} all-to-all(bf16[8,1,12,4096]{3,2,1,0:T(8,128)(2,1)S(1)} %fusion.61), channel_id=1, replica_groups=mesh['sp'=8,'tp'=4] {'sp'}, dimensions={0} | all-to-all | bytes 1572864 | tf_op jit(solution)/shard_map/all_to_all | solution.py:13
  144.3 26.5 %all-gather.2.cloned.1.call-done = bf16[384,4096]{1,0:T(8,128)(2,1)} async-done(((bf16[96,4096]{1,0:T(8,128)(2,1)}), bf16[384,4096]{1,0:T(8,128)(2,1)}) %all-gather.2.cloned.1.call-update) | async-done | bytes 3145744 | tf_op jit(solution)/shard_map/all_gather | solution.py:137
  170.8 3.5 %fusion.26 = f32[384,256]{1,0:T(8,128)S(1)} fusion(bf16[384,4096]{1,0:T(8,128)(2,1)} %all-gather.2.cloned.1.call-done, bf16[1,4096,256]{2,1,0:T(8,128)(2,1)} %param.24), kind=kOutput, calls=%fused_computation.40 | convolution fusion | flops 805306368 | bytes 5636096 | tf_op jit(solution)/shard_map/dot_general | solution.py:138
  174.3 7.7 %convolution_convert_fusion = bf16[384,4096]{1,0:T(8,128)(2,1)} fusion(bf16[1,256,4096]{2,1,0:T(8,128)(2,1)S(1)} %copy-done, bf16[384,4096]{1,0:T(8,128)(2,1)} %all-gather.2.cloned.1.call-done, bf16[1,4096,256]{2,1,0:T(8,128)(2,1)} %param.25, f32[384,256]{1,0:T(8,128)S(1)} %fusion.26), kind=kOutput, calls=%fused_computation.35 | convolution fusion | flops 1612775424 | bytes 10878976 | tf_op jit(solution)/shard_map/dot_general | solution.py:143
  182.0 38.0 %reduce-scatter.5.cloned.1.call-done = bf16[96,4096]{1,0:T(8,128)(2,1)} async-done(((bf16[384,4096]{1,0:T(8,128)(2,1)}), bf16[96,4096]{1,0:T(8,128)(2,1)}) %reduce-scatter.5.cloned.1.call-update) | async-done | bytes 786448 | tf_op jit(solution)/shard_map/reduce_scatter | solution.py:142
  220.1 2.2 all_to_all.12
  222.3 5.5 %all-to-all-start.1 = ((bf16[8,12,4096]{2,1,0:T(8,128)(2,1)}), bf16[8,12,4096]{2,1,0:T(8,128)(2,1)}, u32[]{:S(2)}, u32[]{:S(2)}) async-start(bf16[8,12,4096]{2,1,0:T(8,128)(2,1)} %all_to_all.12), calls=%async_computation.3 | async-start | bytes 2097152 | tf_op jit(solution)/shard_map/all_to_all | solution.py:148
  228.1 25.5 %all-to-all-done.1 = bf16[8,12,4096]{2,1,0:T(8,128)(2,1)} async-done(((bf16[8,12,4096]{2,1,0:T(8,128)(2,1)}), bf16[8,12,4096]{2,1,0:T(8,128)(2,1)}, u32[]{:S(2)}, u32[]{:S(2)}) %all-to-all-start.1) | async-done | bytes 786464 | tf_op jit(solution)/shard_map/all_to_all | solution.py:148
  258.3 1.9 fusion.42
  (121 shorter events, 36.7 us)
Async XLA Ops:
  6.5 167.8 %copy-start = (bf16[1,256,4096]{2,1,0:T(8,128)(2,1)S(1)}, bf16[1,256,4096]{2,1,0:T(8,128)(2,1)}, u32[]{:S(2)}) copy-start(bf16[1,256,4096]{2,1,0:T(8,128)(2,1)} %param.26) | copy-start | bytes 6291460
  6.5 5.9 %copy-start.6 = (f32[4]{0:T(128)S(1)}, f32[4]{0:T(128)}, u32[]{:S(2)}) copy-start(f32[4]{0:T(128)} %param.18) | copy-start | bytes 52
  6.5 101.3 %reduce-scatter.3.cloned.1.call-start = ((), (), s32[]{:S(2)}) async-start(), calls=%async_computation.4 | async-start | bytes 1310720 | tf_op jit(solution)/shard_map/reduce_scatter | solution.py:110
  12.5 6.8 %collective-permute-start = (bf16[2,128,128]{2,1,0:T(8,128)(2,1)S(1)}, bf16[2,128,128]{2,1,0:T(8,128)(2,1)S(1)}, u32[]{:S(2)}, u32[]{:S(2)}) collective-permute-start(bf16[2,128,128]{2,1,0:T(8,128)(2,1)S(1)} %get-tuple-element.299), channel_id=1, source_target_pairs={{0,4},{4,8},{8,12},{12,16},{16,20},{20,24},{24,28},{1,5},{5,9},{9,... | collective-permute-start | bytes 196616 | tf_op jit(solution)/shard_map/while/body/eval_jaxpr/ppermute | solution.py:20
  21.3 6.2 %collective-permute-start = (bf16[2,128,128]{2,1,0:T(8,128)(2,1)S(1)}, bf16[2,128,128]{2,1,0:T(8,128)(2,1)S(1)}, u32[]{:S(2)}, u32[]{:S(2)}) collective-permute-start(bf16[2,128,128]{2,1,0:T(8,128)(2,1)S(1)} %get-tuple-element.299), channel_id=1, source_target_pairs={{0,4},{4,8},{8,12},{12,16},{16,20},{20,24},{24,28},{1,5},{5,9},{9,... | collective-permute-start | bytes 196616 | tf_op jit(solution)/shard_map/while/body/eval_jaxpr/ppermute | solution.py:20
  29.6 6.2 %collective-permute-start = (bf16[2,128,128]{2,1,0:T(8,128)(2,1)S(1)}, bf16[2,128,128]{2,1,0:T(8,128)(2,1)S(1)}, u32[]{:S(2)}, u32[]{:S(2)}) collective-permute-start(bf16[2,128,128]{2,1,0:T(8,128)(2,1)S(1)} %get-tuple-element.299), channel_id=1, source_target_pairs={{0,4},{4,8},{8,12},{12,16},{16,20},{20,24},{24,28},{1,5},{5,9},{9,... | collective-permute-start | bytes 196616 | tf_op jit(solution)/shard_map/while/body/eval_jaxpr/ppermute | solution.py:20
  38.0 7.1 %collective-permute-start = (bf16[2,128,128]{2,1,0:T(8,128)(2,1)S(1)}, bf16[2,128,128]{2,1,0:T(8,128)(2,1)S(1)}, u32[]{:S(2)}, u32[]{:S(2)}) collective-permute-start(bf16[2,128,128]{2,1,0:T(8,128)(2,1)S(1)} %get-tuple-element.299), channel_id=1, source_target_pairs={{0,4},{4,8},{8,12},{12,16},{16,20},{20,24},{24,28},{1,5},{5,9},{9,... | collective-permute-start | bytes 196616 | tf_op jit(solution)/shard_map/while/body/eval_jaxpr/ppermute | solution.py:20
  47.2 7.1 %collective-permute-start = (bf16[2,128,128]{2,1,0:T(8,128)(2,1)S(1)}, bf16[2,128,128]{2,1,0:T(8,128)(2,1)S(1)}, u32[]{:S(2)}, u32[]{:S(2)}) collective-permute-start(bf16[2,128,128]{2,1,0:T(8,128)(2,1)S(1)} %get-tuple-element.299), channel_id=1, source_target_pairs={{0,4},{4,8},{8,12},{12,16},{16,20},{20,24},{24,28},{1,5},{5,9},{9,... | collective-permute-start | bytes 196616 | tf_op jit(solution)/shard_map/while/body/eval_jaxpr/ppermute | solution.py:20
  56.4 7.1 %collective-permute-start = (bf16[2,128,128]{2,1,0:T(8,128)(2,1)S(1)}, bf16[2,128,128]{2,1,0:T(8,128)(2,1)S(1)}, u32[]{:S(2)}, u32[]{:S(2)}) collective-permute-start(bf16[2,128,128]{2,1,0:T(8,128)(2,1)S(1)} %get-tuple-element.299), channel_id=1, source_target_pairs={{0,4},{4,8},{8,12},{12,16},{16,20},{20,24},{24,28},{1,5},{5,9},{9,... | collective-permute-start | bytes 196616 | tf_op jit(solution)/shard_map/while/body/eval_jaxpr/ppermute | solution.py:20
  65.5 7.1 %collective-permute-start = (bf16[2,128,128]{2,1,0:T(8,128)(2,1)S(1)}, bf16[2,128,128]{2,1,0:T(8,128)(2,1)S(1)}, u32[]{:S(2)}, u32[]{:S(2)}) collective-permute-start(bf16[2,128,128]{2,1,0:T(8,128)(2,1)S(1)} %get-tuple-element.299), channel_id=1, source_target_pairs={{0,4},{4,8},{8,12},{12,16},{16,20},{20,24},{24,28},{1,5},{5,9},{9,... | collective-permute-start | bytes 196616 | tf_op jit(solution)/shard_map/while/body/eval_jaxpr/ppermute | solution.py:20
  75.0 4.1 %copy-start.4 = (s32[128,2]{0,1:T(2,128)S(1)}, s32[128,2]{0,1:T(2,128)}, u32[]{:S(2)}) copy-start(s32[128,2]{0,1:T(2,128)} %param.22) | copy-start | bytes 3076
  75.1 32.8 %copy-start.1 = (bf16[32,4096]{1,0:T(8,128)(2,1)S(1)}, bf16[32,4096]{1,0:T(8,128)(2,1)}, u32[]{:S(2)}) copy-start(bf16[32,4096]{1,0:T(8,128)(2,1)} %param.19) | copy-start | bytes 786436
  75.1 33.9 %copy-start.2 = (f32[4096]{0:T(1024)S(1)}, f32[4096]{0:T(1024)}, u32[]{:S(2)}) copy-start(f32[4096]{0:T(1024)} %param.21) | copy-start | bytes 49156
  79.1 91.7 %all-gather.2.cloned.1.call-start = ((), (), s32[]{:S(2)}) async-start(), calls=%async_computation.5 | async-start | bytes 3932160 | tf_op jit(solution)/shard_map/all_gather | solution.py:137
  144.1 76.0 %reduce-scatter.5.cloned.1.call-start = ((), (), s32[]{:S(2)}) async-start(), calls=%async_computation.6 | async-start | bytes 3932160 | tf_op jit(solution)/shard_map/reduce_scatter | solution.py:142
  182.0 45.8 %copy-start.5 = (f32[128]{0:T(128)S(1)}, f32[128]{0:T(128)}, u32[]{:S(2)}) copy-start(f32[128]{0:T(128)} %param.23) | copy-start | bytes 1540
  222.3 31.3 %all-to-all-start.1 = ((bf16[8,12,4096]{2,1,0:T(8,128)(2,1)}), bf16[8,12,4096]{2,1,0:T(8,128)(2,1)}, u32[]{:S(2)}, u32[]{:S(2)}) async-start(bf16[8,12,4096]{2,1,0:T(8,128)(2,1)} %all_to_all.12), calls=%async_computation.3 | async-start | bytes 2097152 | tf_op jit(solution)/shard_map/all_to_all | solution.py:148
  228.1 30.2 %copy-start.3 = (f32[4096]{0:T(1024)S(1)}, f32[4096]{0:T(1024)}, u32[]{:S(2)}) copy-start(f32[4096]{0:T(1024)} %param.27) | copy-start | bytes 49156
Sparse Core Ops, SparseCore 0:
  79.2 28.5 reduce-scatter.2
  144.2 26.5 all-gather.1
  182.2 37.8 reduce-scatter.4
